TPU v7x, 32 devices: a whole 2x2x4 slice. The times are simulated.
32 devices in a mesh: grp: 2 (over x), ep: 16 (over z, y, core), tp: 1.
Axes of the slice: x: 2, y: 2, z: 4, core: 2. Of those that a mesh axis runs over, the one named last changes fastest.
Arguments:
- tokens: bfloat16 [2048, 2048], P(('grp', 'ep')), parts along dimension 0, may hold values from -6 to 6
- norm_gain: float32 [2048], replicated, may hold values from 0.1 to 1.9
- expert_gate: bfloat16 [16, 2048, 512], P('ep', None, 'tp'), may hold values from -0.125 to 0.125
- expert_up: bfloat16 [16, 2048, 512], P('ep', None, 'tp'), may hold values from -0.125 to 0.125
- expert_down: bfloat16 [16, 512, 2048], P('ep', 'tp'), may hold values from -0.25 to 0.25
- shared_gate: bfloat16 [2048, 512], P(None, 'tp'), may hold values from -0.125 to 0.125
- shared_up: bfloat16 [2048, 512], P(None, 'tp'), may hold values from -0.125 to 0.125
- shared_down: bfloat16 [512, 2048], P('tp'), may hold values from -0.25 to 0.25
- routes: int32 [2048, 8], P(('grp', 'ep')), parts along dimension 0, may hold values from 0 to 15, all different within a row; in each aligned block of 64 rows (0 to 63, 64 to 127, ...) at most 64 rows name the same one
- route_weights: float32 [2048, 8], P(('grp', 'ep')), parts along dimension 0, may hold values from 0.05 to 0.6
Outputs:
- mixed: bfloat16 [2048, 2048], P(('grp', 'ep'), 'tp'), parts along dimension 0
There are 2 independent parts, one for each index of `grp`. A program takes and returns all parts, laid end to end along the dimension named above; an argument that names none is the same for every part. Nothing has to cross between parts.
Inputs may be any that keep to these rules, and one draw needn't show every extreme that they name: `routes`: each row names 8 different experts. Within the rows of one index of ep no expert is named more than 64 times, a bound that some block reaches by the rows of some index of ep.
All inputs are finite; a program needn't handle non-finite values.
Results may differ from a plain program's by a relative error of at most 0.0085.
Values may be sent and summed in bfloat16 or wider, within the bound.
A program may use at most 64 MiB of HBM per device.

v0:
```python
import jax
import jax.numpy as jnp
from jax import lax
from jax.sharding import PartitionSpec as P


def rms_scaled(values, gain):
    wide = values.astype(jnp.float32)
    scaled = wide * lax.rsqrt(jnp.mean(wide * wide, axis=-1, keepdims=True) + 1e-06)
    return (scaled * gain).astype(jnp.bfloat16)


def swiglu_partial(row_block, w_gate, w_up, w_down):
    gate_proj = jnp.dot(row_block, w_gate, preferred_element_type=jnp.float32)
    up_proj = jnp.dot(row_block, w_up, preferred_element_type=jnp.float32)
    hidden = (jax.nn.silu(gate_proj) * up_proj).astype(jnp.bfloat16)
    partial_value = jnp.dot(hidden, w_down, preferred_element_type=jnp.float32)
    return lax.optimization_barrier(partial_value.astype(jnp.bfloat16)).astype(jnp.float32)


def per_device(
    tokens,
    norm_gain,
    expert_gate,
    expert_up,
    expert_down,
    shared_gate,
    shared_up,
    shared_down,
    routes,
    route_weights,
):
    tok_rows = tokens.shape[0]
    model_width = tokens.shape[1]
    top_count = routes.shape[1]
    experts = lax.axis_size("ep")
    half_width = model_width // lax.axis_size("tp")
    capacity = min(tok_rows, 2 * tok_rows * top_count // experts)
    normed = rms_scaled(tokens, norm_gain)
    shared_part = swiglu_partial(normed, shared_gate, shared_up, shared_down)
    all_normed = lax.all_gather(normed, "ep", axis=0, tiled=True)
    all_routes = lax.all_gather(routes, "ep", axis=0, tiled=True)
    all_weights = lax.all_gather(route_weights, "ep", axis=0, tiled=True)
    own_expert = lax.axis_index("ep")
    hit_table = all_routes == own_expert
    is_mine = jnp.sum(hit_table.astype(jnp.int32), axis=1).reshape(experts, tok_rows)
    weight_mine = jnp.sum(jnp.where(hit_table, all_weights, jnp.float32(0.0)), axis=1).reshape(
        experts, tok_rows
    )
    slot_rank = jnp.cumsum(is_mine, axis=1) - is_mine
    matches = (slot_rank[:, None, :] == jnp.arange(capacity, dtype=jnp.int32)[None, :, None]) & (
        is_mine[:, None, :] == 1
    )
    slot_token = jnp.sum(
        jnp.where(matches, jnp.arange(tok_rows, dtype=jnp.int32)[None, None, :], 0), axis=2
    )
    slot_live = jnp.any(matches, axis=2).reshape(-1)
    slot_weight = jnp.sum(
        jnp.where(matches, weight_mine[:, None, :], jnp.float32(0.0)), axis=2
    ).reshape(-1)
    global_row = (jnp.arange(experts, dtype=jnp.int32)[:, None] * tok_rows + slot_token).reshape(-1)
    taken = jnp.take(all_normed, global_row, axis=0)
    inbound = jnp.where(slot_live[:, None], taken, jnp.zeros_like(taken))
    expert_part = swiglu_partial(inbound, expert_gate[0], expert_up[0], expert_down[0])
    expert_sum, shared_sum = (
        lax.psum_scatter(
            expert_part.astype(jnp.bfloat16), "tp", scatter_dimension=1, tiled=True
        ).astype(jnp.float32),
        lax.psum_scatter(
            shared_part.astype(jnp.bfloat16), "tp", scatter_dimension=1, tiled=True
        ).astype(jnp.float32),
    )
    expert_out = expert_sum.astype(jnp.bfloat16)
    shared_out = shared_sum.astype(jnp.bfloat16)
    weighted_rows = expert_out.astype(jnp.float32) * slot_weight[:, None]
    terms = (
        jnp.zeros((experts * tok_rows, half_width), jnp.float32).at[global_row].add(weighted_rows)
    )
    routed = lax.psum_scatter(terms, "ep", scatter_dimension=0, tiled=True)
    return (routed + shared_out.astype(jnp.float32)).astype(jnp.bfloat16)


def solution(mesh):
    in_specs = (
        P(("grp", "ep"), None),
        P(),
        P("ep", None, "tp"),
        P("ep", None, "tp"),
        P("ep", "tp", None),
        P(None, "tp"),
        P(None, "tp"),
        P("tp", None),
        P(("grp", "ep"), None),
        P(("grp", "ep"), None),
    )
    out_specs = P(("grp", "ep"), "tp")
    return jax.shard_map(
        per_device, mesh=mesh, in_specs=in_specs, out_specs=out_specs, check_vma=False
    )
```

profile of v0, /device:TPU:0, one launch (start us, length us, event | category | flops | bytes accessed | tf_op | source)
XLA Modules:
  0.0 220.2 jit_solution(10762716393236686828)
XLA Ops:
  6.5 0.0 copy-start
  6.5 0.0 all-gather.4.cloned.1.call-start
  6.5 1.2 fusion.15
  7.8 1.8 fusion.17
  9.6 0.0 all-gather.4.cloned.1.call-update
  9.6 0.0 reduce-scatter.2.cloned.1.call-start
  9.7 23.8 %all-gather = s32[16,64,8]{1,2,0:T(8,128)S(1)} all-gather(s32[1,64,8]{1,2,0:T(8,128)} %bitcast.23), channel_id=1, replica_groups=mesh['grp'=2,'ep'=16,'tp'=1] {'ep'}, dimensions={0}, use_global_device_ids=true | all-gather | bytes 34816 | tf_op jit(solution)/shard_map/all_gather | solution.py:42
  33.4 18.4 %all-gather.1 = f32[16,64,8]{1,2,0:T(8,128)S(1)} all-gather(f32[1,64,8]{1,2,0:T(8,128)} %bitcast.24), channel_id=1, replica_groups=mesh['grp'=2,'ep'=16,'tp'=1] {'ep'}, dimensions={0}, use_global_device_ids=true | all-gather | bytes 34816 | tf_op jit(solution)/shard_map/all_gather | solution.py:43
  51.9 0.2 reduce_window_sum.14
  52.1 0.4 select_reduce_fusion.1
  52.5 0.1 broadcast_add_fusion
  52.5 0.1 add.80
  52.6 0.1 add.77
  52.7 0.2 select_reduce_fusion
  52.9 0.1 mul.59
  53.0 0.4 fusion.19
  53.3 0.1 broadcast_in_dim.66
  53.5 9.7 %all-gather.4.cloned.1.call-done = bf16[1024,2048]{1,0:T(8,128)(2,1)} async-done(((bf16[64,2048]{1,0:T(8,128)(2,1)}), bf16[1024,2048]{1,0:T(8,128)(2,1)}) %all-gather.4.cloned.1.call-update) | async-done | bytes 4194320 | tf_op jit(solution)/shard_map/all_gather | solution.py:41
  63.2 11.7 %gather_fusion = bf16[1024,2048]{1,0:T(8,128)(2,1)} fusion(bf16[1024,2048]{1,0:T(8,128)(2,1)} %all-gather.4.cloned.1.call-done, s32[1024]{0:T(1024)S(1)} %broadcast_clamp_fusion), kind=kCustom, calls=%fused_computation | custom fusion | bytes 8392704 | tf_op jit(solution)/shard_map/jit(_take)/gather | solution.py:62
  75.0 6.6 %fusion.6 = f32[1024,512]{1,0:T(8,128)} fusion(bf16[1,2048,512]{2,1,0:T(8,128)(2,1)} %param.13, bf16[1024,2048]{1,0:T(8,128)(2,1)} %gather_fusion, pred[1024]{0:T(1024)(128)(4,1)S(1)} %compare_and_fusion, pred[1024]{0:T(1024)(128)(4,1)S(1)} %broadcast_in_dim.66), kind=kOutput, calls=%fused_computation.11 | convolution fusion | flops 2151677952 | bytes 8390656 | tf_op jit(solution)/shard_map/dot_general | solution.py:15
  81.5 0.0 copy-done
  81.5 9.2 %convolution_convert_fusion = bf16[1024,2048]{1,0:T(8,128)(2,1)} fusion(bf16[1,512,2048]{2,1,0:T(8,128)(2,1)S(1)} %copy-done, f32[1024,512]{1,0:T(8,128)} %fusion.6, bf16[1,2048,512]{2,1,0:T(8,128)(2,1)} %param.12, bf16[1024,2048]{1,0:T(8,128)(2,1)} %gather_fusion, pred[1024]{0:T(1024)(128)(4,1)S(1)} %compare_and_fusion, ...), kind=kOutput, calls=%fused_computation.8 | convolution fusion | flops 4304404480 | bytes 14682112 | tf_op jit(solution)/shard_map/dot_general | solution.py:17
  90.7 18.6 %scatter_custom_fusion = f32[1024,2048]{1,0:T(8,128)} fusion(s32[1024]{0:T(1024)S(1)} %bitcast.22, bf16[1024,2048]{1,0:T(8,128)(2,1)} %convolution_convert_fusion, f32[1024]{0:T(1024)S(1)} %mul.59, f32[]{:T(128)} %constant.13.clone.1), kind=kCustom, calls=%fused_computation.2 | custom fusion | flops 6291456 | bytes 12587012 | tf_op jit(solution)/shard_map/scatter-add | solution.py:77
  109.3 0.0 copy-start.1
  109.3 0.0 reduce-scatter.2.cloned.1.call-update
  109.4 0.9 copy-done.1
  110.3 2.1 fusion.28
  112.4 3.5 %convolution_convert_fusion.1 = bf16[64,2048]{1,0:T(8,128)(2,1)S(1)} fusion(bf16[512,2048]{1,0:T(8,128)(2,1)} %param.17, bf16[64,2048]{1,0:T(8,128)(2,1)S(1)} %copy-done.1, bf16[2048,512]{1,0:T(8,128)(2,1)} %param.16, f32[64,512]{1,0:T(8,128)S(1)} %fusion.28), kind=kOutput, calls=%fused_computation.9 | convolution fusion | flops 268763136 | bytes 4849664 | tf_op jit(solution)/shard_map/dot_general | solution.py:17
  115.9 95.8 %reduce-scatter.2.cloned.1.call-done = f32[64,2048]{1,0:T(8,128)} async-done(((f32[1024,2048]{1,0:T(8,128)}), f32[64,2048]{1,0:T(8,128)}) %reduce-scatter.2.cloned.1.call-update) | async-done | bytes 524304 | tf_op jit(solution)/shard_map/reduce_scatter | solution.py:79
  211.6 1.8 add_convert_fusion
  (9 shorter events, 0.1 us)
Async XLA Ops:
  6.5 75.0 %copy-start = (bf16[1,512,2048]{2,1,0:T(8,128)(2,1)S(1)}, bf16[1,512,2048]{2,1,0:T(8,128)(2,1)}, u32[]{:S(2)}) copy-start(bf16[1,512,2048]{2,1,0:T(8,128)(2,1)} %param.14) | copy-start | bytes 6291460
  6.5 56.7 %all-gather.4.cloned.1.call-start = ((), (), s32[]{:S(2)}) async-start(), calls=%async_computation.1 | async-start | bytes 4456448 | tf_op jit(solution)/shard_map/all_gather | solution.py:41
  9.6 202.0 %reduce-scatter.2.cloned.1.call-start = ((), (), s32[]{:S(2)}) async-start(), calls=%async_computation.2 | async-start | bytes 8912896 | tf_op jit(solution)/shard_map/reduce_scatter | solution.py:79
  109.3 0.9 copy-start.1
Sparse Core Ops, SparseCore 0:
  9.7 53.4 all-gather.3
  109.5 102.0 reduce-scatter.1
where the time goes:
time: 221 us; the launch traced here: 220 us
  waiting for transfers between devices  106 us (48%)
  blocking collectives  42.1 us (19%)
  other arithmetic  24.8 us (11%)
  matrix products  21.3 us (10%)
  between operations  13.5 us (6%)
  local copies, waits for them, and re-layouts  13 us (6%)
    reduce_scatter x1, waiting for transfers between devices, per_device(): routed = lax.psum_scatter(terms, 'ep', scatter_dimension=0, tiled=True)  95.8 us
    all_gather x1, blocking collectives, per_device(): all_routes = lax.all_gather(routes, 'ep', axis=0, tiled=True)  23.8 us
    scatter-add x1, other arithmetic, per_device(): jnp.zeros((experts * tok_rows, half_width), jnp.float32).at[global_row]  18.6 us
    all_gather x1, blocking collectives, per_device(): all_weights = lax.all_gather(route_weights, 'ep', axis=0, tiled=True)  18.4 us
    dot_general x2, matrix products, swiglu_partial(): partial_value = jnp.dot(hidden, w_down, preferred_element_type=jnp.float32)  12.7 us
    gather x1, local copies, waits for them, and re-layouts, per_device(): taken = jnp.take(all_normed, global_row, axis=0)  11.7 us
    all_gather x1, waiting for transfers between devices, per_device(): all_normed = lax.all_gather(normed, 'ep', axis=0, tiled=True)  9.75 us
    dot_general x1, matrix products, swiglu_partial(): up_proj = jnp.dot(row_block, w_up, preferred_element_type=jnp.float32)  6.57 us
  transfers between devices with their start and end apart: 2, of which 2 were waited for; matrix products, arithmetic and copies ran while one was open for 3% of the time, Pallas kernels for 0%

commit v1 on v0

--- a/solution.py
+++ b/solution.py
@@ -39,8 +39,11 @@
     normed = rms_scaled(tokens, norm_gain)
     shared_part = swiglu_partial(normed, shared_gate, shared_up, shared_down)
     all_normed = lax.all_gather(normed, "ep", axis=0, tiled=True)
-    all_routes = lax.all_gather(routes, "ep", axis=0, tiled=True)
-    all_weights = lax.all_gather(route_weights, "ep", axis=0, tiled=True)
+    all_routes, all_weights = jnp.split(
+        lax.all_gather(jnp.concatenate([routes, route_weights], axis=1), "ep", axis=0, tiled=True),
+        [routes.shape[1]],
+        axis=1,
+    )
     own_expert = lax.axis_index("ep")
     hit_table = all_routes == own_expert
     is_mine = jnp.sum(hit_table.astype(jnp.int32), axis=1).reshape(experts, tok_rows)

time: 221 us -> 220 us (level)
  blocking collectives: 42.1 us -> 23.7 us
  waiting for transfers between devices: 106 us -> 122 us
    all_gather x2 -> x1, blocking collectives: 42.1 us -> 23.7 us  [per_device(): lax.all_gather(jnp.concatenate([routes, route_weights], axis=1), 'ep', ax...]
    all_gather x1, waiting for transfers between devices: 9.75 us -> 26.2 us  [per_device(): all_normed = lax.all_gather(normed, 'ep', axis=0, tiled=True)]
  transfers between devices with their start and end apart: 2 -> 2, of which waited for: 2 -> 2; matrix products, arithmetic and copies ran while one was open for 3% -> 4% of each run, Pallas kernels for 0% -> 0%
where the time goes in v1:
time: 220 us
  waiting for transfers between devices  122 us (55%)
  other arithmetic  26.1 us (12%)
  blocking collectives  23.7 us (11%)
  matrix products  21.3 us (10%)
  between operations  13.5 us (6%)
  local copies, waits for them, and re-layouts  13.3 us (6%)
    reduce_scatter x1, waiting for transfers between devices, per_device(): routed = lax.psum_scatter(terms, 'ep', scatter_dimension=0, tiled=True)  95.6 us
    all_gather x1, waiting for transfers between devices, per_device(): all_normed = lax.all_gather(normed, 'ep', axis=0, tiled=True)  26.2 us
    all_gather x1, blocking collectives, per_device(): lax.all_gather(jnp.concatenate([routes, route_weights], axis=1), 'ep', ax...  23.7 us
    scatter-add x1, other arithmetic, per_device(): jnp.zeros((experts * tok_rows, half_width), jnp.float32).at[global_row]  18.6 us
    dot_general x2, matrix products, swiglu_partial(): partial_value = jnp.dot(hidden, w_down, preferred_element_type=jnp.float32)  12.7 us
    gather x1, local copies, waits for them, and re-layouts, per_device(): taken = jnp.take(all_normed, global_row, axis=0)  11.7 us
    dot_general x1, matrix products, swiglu_partial(): up_proj = jnp.dot(row_block, w_up, preferred_element_type=jnp.float32)  6.58 us
  transfers between devices with their start and end apart: 2, of which 2 were waited for; matrix products, arithmetic and copies ran while one was open for 4% of the time, Pallas kernels for 0%

profile of v1, /device:TPU:0, one launch (start us, length us, event | category | flops | bytes accessed | tf_op | source)
XLA Modules:
  0.0 219.9 jit_solution(17964895184227281096)
XLA Ops:
  6.5 0.0 copy-start
  6.5 0.0 all-gather.3.cloned.1.call-start
  6.5 1.2 fusion.15
  7.8 1.8 fusion.17
  9.6 0.0 all-gather.3.cloned.1.call-update
  9.6 0.0 reduce-scatter.2.cloned.1.call-start
  9.7 0.7 convert_element_type.44
  10.4 0.7 maximum_bitcast_fusion
  11.1 23.7 %all-gather = f32[16,64,16]{1,2,0:T(8,128)S(1)} all-gather(f32[1,64,16]{1,2,0:T(8,128)S(1)} %maximum_bitcast_fusion), channel_id=1, replica_groups=mesh['grp'=2,'ep'=16,'tp'=1] {'ep'}, dimensions={0}, use_global_device_ids=true | all-gather | bytes 69632 | tf_op jit(solution)/shard_map/all_gather | solution.py:43
  34.8 0.1 reshape.93
  35.0 0.1 reduce_window_sum.13
  35.0 0.2 reduce_window_sum.14
  35.3 0.4 select_reduce_fusion.1
  35.6 0.1 broadcast_add_fusion
  35.7 0.1 add.80
  35.8 0.1 add.77
  35.9 0.1 broadcast_in_dim.72
  35.9 0.2 select_reduce_fusion
  36.2 0.1 mul.59
  36.2 0.4 fusion.19
  36.6 0.1 broadcast_in_dim.66
  36.7 26.2 %all-gather.3.cloned.1.call-done = bf16[1024,2048]{1,0:T(8,128)(2,1)} async-done(((bf16[64,2048]{1,0:T(8,128)(2,1)}), bf16[1024,2048]{1,0:T(8,128)(2,1)}) %all-gather.3.cloned.1.call-update) | async-done | bytes 4194320 | tf_op jit(solution)/shard_map/all_gather | solution.py:41
  63.0 11.7 %gather_fusion = bf16[1024,2048]{1,0:T(8,128)(2,1)} fusion(bf16[1024,2048]{1,0:T(8,128)(2,1)} %all-gather.3.cloned.1.call-done, s32[1024]{0:T(1024)S(1)} %broadcast_clamp_fusion), kind=kCustom, calls=%fused_computation | custom fusion | bytes 8392704 | tf_op jit(solution)/shard_map/jit(_take)/gather | solution.py:65
  74.7 6.6 %fusion.6 = f32[1024,512]{1,0:T(8,128)} fusion(bf16[1,2048,512]{2,1,0:T(8,128)(2,1)} %param.13, bf16[1024,2048]{1,0:T(8,128)(2,1)} %gather_fusion, pred[1024]{0:T(1024)(128)(4,1)S(1)} %compare_and_fusion, pred[1024]{0:T(1024)(128)(4,1)S(1)} %broadcast_in_dim.66), kind=kOutput, calls=%fused_computation.11 | convolution fusion | flops 2151677952 | bytes 8390656 | tf_op jit(solution)/shard_map/dot_general | solution.py:15
  81.3 0.0 copy-done
  81.3 9.2 %convolution_convert_fusion = bf16[1024,2048]{1,0:T(8,128)(2,1)} fusion(bf16[1,512,2048]{2,1,0:T(8,128)(2,1)S(1)} %copy-done, f32[1024,512]{1,0:T(8,128)} %fusion.6, bf16[1,2048,512]{2,1,0:T(8,128)(2,1)} %param.12, bf16[1024,2048]{1,0:T(8,128)(2,1)} %gather_fusion, pred[1024]{0:T(1024)(128)(4,1)S(1)} %compare_and_fusion, ...), kind=kOutput, calls=%fused_computation.8 | convolution fusion | flops 4304404480 | bytes 14682112 | tf_op jit(solution)/shard_map/dot_general | solution.py:17
  90.5 18.6 %scatter_custom_fusion = f32[1024,2048]{1,0:T(8,128)} fusion(s32[1024]{0:T(1024)S(1)} %bitcast.24, bf16[1024,2048]{1,0:T(8,128)(2,1)} %convolution_convert_fusion, f32[1024]{0:T(1024)S(1)} %mul.59, f32[]{:T(128)} %constant.13.clone.1), kind=kCustom, calls=%fused_computation.2 | custom fusion | flops 6291456 | bytes 12587012 | tf_op jit(solution)/shard_map/scatter-add | solution.py:80
  109.1 0.0 copy-start.1
  109.1 0.0 reduce-scatter.2.cloned.1.call-update
  109.1 0.9 copy-done.1
  110.0 2.1 fusion.29
  112.1 3.5 %convolution_convert_fusion.1 = bf16[64,2048]{1,0:T(8,128)(2,1)S(1)} fusion(bf16[512,2048]{1,0:T(8,128)(2,1)} %param.17, bf16[64,2048]{1,0:T(8,128)(2,1)S(1)} %copy-done.1, bf16[2048,512]{1,0:T(8,128)(2,1)} %param.16, f32[64,512]{1,0:T(8,128)S(1)} %fusion.29), kind=kOutput, calls=%fused_computation.9 | convolution fusion | flops 268763136 | bytes 4849664 | tf_op jit(solution)/shard_map/dot_general | solution.py:17
  115.6 95.6 %reduce-scatter.2.cloned.1.call-done = f32[64,2048]{1,0:T(8,128)} async-done(((f32[1024,2048]{1,0:T(8,128)}), f32[64,2048]{1,0:T(8,128)}) %reduce-scatter.2.cloned.1.call-update) | async-done | bytes 524304 | tf_op jit(solution)/shard_map/reduce_scatter | solution.py:82
  211.2 1.8 add_convert_fusion
  (10 shorter events, 0.1 us)
Async XLA Ops:
  6.5 74.7 %copy-start = (bf16[1,512,2048]{2,1,0:T(8,128)(2,1)S(1)}, bf16[1,512,2048]{2,1,0:T(8,128)(2,1)}, u32[]{:S(2)}) copy-start(bf16[1,512,2048]{2,1,0:T(8,128)(2,1)} %param.14) | copy-start | bytes 6291460
  6.5 56.4 %all-gather.3.cloned.1.call-start = ((), (), s32[]{:S(2)}) async-start(), calls=%async_computation.1 | async-start | bytes 4456448 | tf_op jit(solution)/shard_map/all_gather | solution.py:41
  9.6 201.6 %reduce-scatter.2.cloned.1.call-start = ((), (), s32[]{:S(2)}) async-start(), calls=%async_computation.2 | async-start | bytes 8912896 | tf_op jit(solution)/shard_map/reduce_scatter | solution.py:82
  109.1 0.9 copy-start.1
Sparse Core Ops, SparseCore 0:
  9.7 53.1 all-gather.2
  109.2 101.9 reduce-scatter.1
